TPU v7x, 768 devices: a whole 4x8x12 slice. The times are simulated.
768 devices in a mesh: sp: 96 (over z, y), tp: 8 (over x, core).
Axes of the slice: x: 4, y: 8, z: 12, core: 2. Of those that a mesh axis runs over, the one named last changes fastest.
Arguments:
- tokens: bfloat16 [18432, 2048], P(('sp', 'tp')), may hold values from -6 to 6
- norm_in: float32 [2048], replicated, may hold values from 0.1 to 1.9
- decay_log: float32 [128, 64], P('tp'), may hold values from -0.034 to -1.3563368e-05, as said below
- phase: float32 [128, 64], P('tp'), may hold values from -1 to 1
- b_real: float32 [128, 64, 16], P('tp'), may hold values from -1 to 1
- b_imag: float32 [128, 64, 16], P('tp'), may hold values from -1 to 1
- c_real: float32 [128, 16, 64], P('tp'), may hold values from -0.75 to 0.75
- c_imag: float32 [128, 16, 64], P('tp'), may hold values from -0.75 to 0.75
- skip_gain: float32 [2048], P('tp'), may hold values from -6 to 6
- w_value: bfloat16 [2048, 2048], P(None, 'tp'), as said below
- w_gate: bfloat16 [2048, 2048], P(None, 'tp'), may hold values from -0.125 to 0.125
- norm_out: float32 [2048], P('tp'), may hold values from 0.1 to 1.9
Outputs:
- mixed: bfloat16 [18432, 2048], P('sp', 'tp')
Inputs may be any that keep to these rules, and one draw needn't show every extreme that they name: `decay_log`: negative real parts of the eigenvalues. `w_value`: weights of the value projection.
All inputs are finite; a program needn't handle non-finite values.
Results may differ from a plain program's by a relative error of at most 0.012.
The roundings to bfloat16 on the way count: a program that leaves them out, or rounds other values in their place, can miss the bound.
Values may be sent and summed in bfloat16 or wider, within the bound.
A program may use at most 32 MiB of HBM per device.

v0:
```python
import jax
import jax.numpy as jnp
from jax import lax
from jax.sharding import Mesh
from jax.sharding import PartitionSpec as P

D = 2048
SP = ("sp_0", "sp_1")
SP_TP = ("sp_0", "sp_1", "tp")


NORM_EPS = 1e-06
HIGHEST_PREC = lax.Precision.HIGHEST


def neutral_like(value, identity):
    return jax.tree.map(
        lambda part, zero: jnp.zeros_like(part) + jnp.asarray(zero, part.dtype), value, identity
    )


def gathered_once(value, axis):
    leaves = jax.tree.leaves(value)
    sequence = sorted(range(len(leaves)), key=lambda k: -leaves[k].size)
    width = (1, *leaves[sequence[0]].shape)[-1]
    lines = [
        jnp.pad(leaves[k].reshape(-1), (0, -leaves[k].size % width)).reshape(-1, width)
        for k in sequence
    ]
    both, at, found = (lax.all_gather(jnp.concatenate(lines), axis), 0, {})
    for k, line in zip(sequence, lines):
        slab = both[:, at : at + len(line)].reshape(len(both), -1)
        found[k] = slab[:, : leaves[k].size].reshape(-1, *leaves[k].shape)
        at += len(line)
    numbers = iter(range(len(leaves)))
    return jax.tree.map(lambda _: found[next(numbers)], value)


def entering(value, axes, combine, identity):
    before = start = neutral_like(value, identity)
    subtotal = value
    for axis in reversed(axes):
        peers, place = (lax.axis_size(axis), lax.axis_index(axis))
        pieces = gathered_once(subtotal, axis)
        inside, subtotal = (start, start)
        for k in range(peers):
            passed = k < place
            subtotal = combine(subtotal, jax.tree.map(lambda part: part[k], pieces))
            inside = jax.tree.map(lambda new, old: jnp.where(passed, new, old), subtotal, inside)
        before = combine(inside, before)
    return before


def joined_along(parts, dim):
    dims = list(parts.shape[1:])
    dims[dim] *= parts.shape[0]
    return jnp.moveaxis(parts, 0, dim).reshape(dims)


def sent_to_all(value, axis):
    peers = lax.axis_size(axis)
    return lax.all_to_all(
        jnp.broadcast_to(value[None], (peers, *value.shape)), axis, 0, 0, tiled=True
    )


def gathered_copies(value, axis, dim):
    return joined_along(sent_to_all(value, axis), dim)


def over_copies(value, axis):
    return sent_to_all(value, axis).sum(axis=0)


def coefficients(decay_log, phase, b_real, b_imag):
    magnitude = jnp.exp(decay_log)
    bar_re = magnitude * jnp.cos(phase)
    bar_im = magnitude * jnp.sin(phase)
    modulus = decay_log * decay_log + phase * phase
    coef_re = ((bar_re - 1.0) * decay_log + bar_im * phase) / modulus
    coef_im = (bar_im * decay_log - (bar_re - 1.0) * phase) / modulus
    in_re = coef_re[:, :, None] * b_real - coef_im[:, :, None] * b_imag
    in_im = coef_re[:, :, None] * b_imag + coef_im[:, :, None] * b_real
    return (bar_re, bar_im, in_re, in_im)


def prefix_states(drive_re, drive_im, rate_re, rate_im):
    length = drive_re.shape[0]
    stride = 1
    for level in range(max(length - 1, 1).bit_length()):
        padding = jnp.zeros((stride,) + drive_re.shape[1:], jnp.float32)
        moved_re = jnp.concatenate([padding, drive_re[: length - stride]], axis=0)
        moved_im = jnp.concatenate([padding, drive_im[: length - stride]], axis=0)
        drive_re, drive_im = (
            drive_re + rate_re * moved_re - rate_im * moved_im,
            drive_im + rate_re * moved_im + rate_im * moved_re,
        )
        rate_re, rate_im = (rate_re * rate_re - rate_im * rate_im, 2.0 * rate_re * rate_im)
        stride = stride * 2
    return (drive_re, drive_im)


def readout(state_re, state_im, c_real, c_imag):
    first = jnp.einsum("tgp,ghp->tgh", state_re, c_real, precision=HIGHEST_PREC)
    second = jnp.einsum("tgp,ghp->tgh", state_im, c_imag, precision=HIGHEST_PREC)
    return first - second


def powers(decay_log, phase, exponents):
    magnitude = jnp.exp(exponents[:, None, None] * decay_log[None])
    angles = exponents[:, None, None] * phase[None]
    return (magnitude * jnp.cos(angles), magnitude * jnp.sin(angles))


def combine(earlier, later):
    first_re, first_im, held_re, held_im = earlier
    second_re, second_im, own_re, own_im = later
    return (
        first_re * second_re - first_im * second_im,
        first_re * second_im + first_im * second_re,
        second_re * held_re - second_im * held_im + own_re,
        second_re * held_im + second_im * held_re + own_im,
    )


def on_device(
    tokens,
    norm_in,
    decay_log,
    phase,
    b_real,
    b_imag,
    c_real,
    c_imag,
    skip_gain,
    w_value,
    w_gate,
    norm_out,
):
    xf = tokens.astype(jnp.float32)
    normed = (xf * lax.rsqrt(jnp.mean(xf * xf, axis=1, keepdims=True) + NORM_EPS) * norm_in).astype(
        jnp.bfloat16
    )
    by_channel = lax.all_to_all(normed, "tp", split_axis=1, concat_axis=0, tiled=True)
    row_total, width = by_channel.shape
    groups = decay_log.shape[0]
    drive = by_channel.astype(jnp.float32).reshape(row_total, groups, width // groups)
    bar_re, bar_im, bb_re, bb_im = coefficients(decay_log, phase, b_real, b_imag)
    in_re = jnp.einsum("tgh,gph->tgp", drive, bb_re, precision=HIGHEST_PREC)
    in_im = jnp.einsum("tgh,gph->tgp", drive, bb_im, precision=HIGHEST_PREC)
    positions = jnp.arange(row_total, dtype=jnp.float32)
    states_re, states_im = prefix_states(in_re, in_im, bar_re, bar_im)
    end_re, end_im = (states_re[-1], states_im[-1])
    whole_re, whole_im = powers(decay_log, phase, jnp.full((1,), row_total, jnp.float32))
    unity = jnp.ones_like(end_re)
    nothing = jnp.zeros_like(end_re)
    carried = entering(
        (whole_re[0], whole_im[0], end_re, end_im), SP, combine, (unity, nothing, nothing, nothing)
    )
    held_re, held_im = (carried[2], carried[3])
    ahead_re, ahead_im = powers(decay_log, phase, positions + 1.0)
    total_re = states_re + ahead_re * held_re - ahead_im * held_im
    total_im = states_im + ahead_re * held_im + ahead_im * held_re
    mixed_pre = readout(total_re, total_im, c_real, c_imag) + skip_gain.reshape(groups, -1) * drive
    z_local = jax.nn.gelu(mixed_pre).reshape(row_total, width).astype(jnp.bfloat16)
    shard_rows = gathered_copies(z_local, "tp", 1)
    projected_value = jnp.dot(shard_rows, w_value, preferred_element_type=jnp.float32)
    projected_gate = jnp.dot(shard_rows, w_gate, preferred_element_type=jnp.float32)
    gated = projected_value * jax.nn.sigmoid(projected_gate)
    squares = over_copies(jnp.sum(gated * gated, axis=1), "tp")
    scale = lax.rsqrt(squares / D + NORM_EPS)
    return (gated * scale[:, None] * norm_out).astype(jnp.bfloat16)


def solution(mesh):
    torus = Mesh(mesh.devices.reshape(12, 8, mesh.shape["tp"]), ("sp_0", "sp_1", "tp"))
    in_specs = (
        P(SP_TP, None),
        P(),
        P("tp", None),
        P("tp", None),
        P("tp", None, None),
        P("tp", None, None),
        P("tp", None, None),
        P("tp", None, None),
        P("tp"),
        P(None, "tp"),
        P(None, "tp"),
        P("tp"),
    )
    out_specs = P(SP, "tp")
    return jax.shard_map(
        on_device, mesh=torus, in_specs=in_specs, out_specs=out_specs, check_vma=False
    )
```

profile of v0, /device:TPU:1, one launch (start us, length us, event | category | flops | bytes accessed | tf_op | source)
XLA Modules:
  0.0 124.1 jit_solution(6091489590401653313)
XLA Ops:
  0.0 0.0 copy-start
  0.0 0.0 copy-start.3
  0.0 1.1 fusion.50
  1.1 0.0 copy-done.3
  1.1 0.8 fusion.52
  1.9 0.6 copy.40
  2.6 13.7 %all-to-all-start = ((bf16[24,8,256]{2,0,1:T(8,128)(2,1)}), bf16[24,8,256]{2,0,1:T(8,128)(2,1)S(1)}, u32[]{:S(2)}, u32[]{:S(2)}) async-start(bf16[24,8,256]{2,0,1:T(8,128)(2,1)} %bitcast.366), calls=%async_computation | async-start | bytes 196608 | tf_op jit(solution)/shard_map/all_to_all | solution.py:144
  16.3 0.0 copy-start.7
  16.3 0.0 copy-start.4
  16.3 0.0 copy-start.5
  16.3 0.7 copy-done.7
  17.0 0.1 mul.1444
  17.1 0.0 copy-done.4
  17.1 0.0 copy-done.5
  17.1 0.1 multiply_subtract_fusion.13
  17.2 4.1 %all-to-all-done = bf16[24,8,256]{2,0,1:T(8,128)(2,1)S(1)} async-done(((bf16[24,8,256]{2,0,1:T(8,128)(2,1)}), bf16[24,8,256]{2,0,1:T(8,128)(2,1)S(1)}, u32[]{:S(2)}, u32[]{:S(2)}) %all-to-all-start) | async-done | bytes 98336 | tf_op jit(solution)/shard_map/all_to_all | solution.py:144
  21.3 0.3 copy.32
  21.6 0.0 copy-start.1
  21.7 0.0 copy-start.2
  21.7 0.3 reshape.93
  22.0 0.5 copy-done.1
  22.5 0.1 copy-done.2
  22.6 0.6 convolution_bitcast_fusion.1
  23.2 0.6 convolution_bitcast_fusion
  23.9 0.9 multiply_add_fusion.5
  24.8 0.9 multiply_add_fusion.4
  25.7 0.9 multiply_add_fusion.3
  26.6 0.9 multiply_add_fusion.2
  27.6 0.9 multiply_add_fusion.1
  28.5 0.9 multiply_add_fusion
  29.5 0.9 fusion.7
  30.5 0.4 fusion.11
  30.9 0.6 slice_reduce_fusion
  31.6 18.8 %all-gather = f32[512,64]{1,0:T(8,128)S(1)} all-gather(f32[64,64]{1,0:T(8,128)S(1)} %pad_maximum_fusion), channel_id=2, replica_groups=mesh['sp_0'=12,'sp_1'=8,'tp'=8] {'sp_1'}, dimensions={0}, use_global_device_ids=true | all-gather | bytes 147456 | tf_op jit(solution)/shard_map/all_gather | solution.py:30
  50.6 23.3 %all-gather.1 = f32[768,64]{1,0:T(8,128)S(1)} all-gather(f32[64,64]{1,0:T(8,128)S(1)} %pad_maximum_fusion.1), channel_id=3, replica_groups=mesh['sp_0'=12,'sp_1'=8,'tp'=8] {'sp_0'}, dimensions={0}, use_global_device_ids=true | all-gather | bytes 212992 | tf_op jit(solution)/shard_map/all_gather | solution.py:30
  73.9 0.0 copy-start.9
  73.9 0.1 add_bitcast_fusion.1
  74.0 0.8 copy-done.9
  74.8 0.0 copy-start.10
  74.8 4.9 %fusion.19 = f32[16,192,16]{1,2,0:T(8,128)S(1)} fusion(f32[16,16,64]{2,1,0:T(8,128)S(1)} %copy-done.9, f32[192,16,64]{0,2,1:T(8,128)S(1)} %get-tuple-element.56, f32[16,64]{1,0:T(8,128)S(1)} %add_bitcast_fusion, f32[16,64]{1,0:T(8,128)S(1)} %get-tuple-element.5, f32[16,64]{1,0:T(8,128)S(1)} %copy-done.4, f32[16,64]{1,0:T(8,128)S(1)} %copy-done.5, ...), kind=kOutput, calls=%fused_computation.34 | convolution fusion | flops 39321600 | bytes 1065728 | tf_op jit(solution)/shard_map/tgp,ghp->tgh/dot_general | solution.py:104
  79.7 0.0 copy-done.10
  79.7 6.5 %fusion.47 = bf16[192,16,16]{0,2,1:T(8,128)(2,1)S(1)} fusion(f32[16,192,16]{1,2,0:T(8,128)S(1)} %fusion.19, f32[16,16,64]{2,1,0:T(8,128)S(1)} %copy-done.10, f32[192,16,64]{0,2,1:T(8,128)S(1)} %get-tuple-element.55, f32[16,64]{1,0:T(8,128)S(1)} %add_bitcast_fusion, f32[16,64]{1,0:T(8,128)S(1)} %get-tuple-element.5, f32[16,64]{1,0:T(8,128)S(1)} %copy-done.4, ...), kind=kOutput, calls=%fused_computation.72 | convolution fusion | flops 39960576 | bytes 1263360 | tf_op jit(solution)/shard_map/tgp,ghp->tgh/dot_general | solution.py:105
  86.2 0.1 copy.33
  86.3 0.1 broadcast_in_dim.10
  86.3 26.2 %all_to_all.27 = bf16[8,192,256]{2,1,0:T(8,128)(2,1)S(1)} all-to-all(bf16[8,192,256]{2,1,0:T(8,128)(2,1)S(1)} %broadcast_in_dim.10), channel_id=1, replica_groups=mesh['sp_0'=12,'sp_1'=8,'tp'=8] {'tp'}, dimensions={0} | all-to-all | bytes 1572864 | tf_op jit(solution)/shard_map/all_to_all | solution.py:62
  112.5 0.0 copy-start.8
  112.5 0.1 copy.38
  112.6 1.1 copy-done.8
  113.8 0.4 fusion.4
  114.2 0.0 copy-done
  114.2 0.5 multiply_reduce_fusion
  114.7 8.0 %all_to_all.28 = f32[8,1,192]{2,1,0:T(1,128)S(1)} all-to-all(f32[8,1,192]{2,1,0:T(1,128)S(1)} %broadcast_in_dim.11), channel_id=1, replica_groups=mesh['sp_0'=12,'sp_1'=8,'tp'=8] {'tp'}, dimensions={0} | all-to-all | bytes 12288 | tf_op jit(solution)/shard_map/all_to_all | solution.py:62
  122.7 0.0 copy-start.6
  122.7 0.7 copy-done.6
  123.4 0.7 multiply_convert_fusion
  (22 shorter events, 0.3 us)
Async XLA Ops:
  0.0 114.2 %copy-start = (bf16[2048,256]{1,0:T(8,128)(2,1)S(1)}, bf16[2048,256]{1,0:T(8,128)(2,1)}, u32[]{:S(2)}) copy-start(bf16[2048,256]{1,0:T(8,128)(2,1)} %param.21) | copy-start | bytes 3145732
  0.0 1.1 copy-start.3
  2.6 18.7 %all-to-all-start = ((bf16[24,8,256]{2,0,1:T(8,128)(2,1)}), bf16[24,8,256]{2,0,1:T(8,128)(2,1)S(1)}, u32[]{:S(2)}, u32[]{:S(2)}) async-start(bf16[24,8,256]{2,0,1:T(8,128)(2,1)} %bitcast.366), calls=%async_computation | async-start | bytes 196608 | tf_op jit(solution)/shard_map/all_to_all | solution.py:144
  16.3 0.7 copy-start.7
  16.3 0.8 copy-start.4
  16.3 0.8 copy-start.5
  21.6 0.9 copy-start.1
  21.7 1.0 copy-start.2
  73.9 0.9 copy-start.9
  74.8 4.9 %copy-start.10 = (f32[16,16,64]{2,1,0:T(8,128)S(1)}, f32[16,16,64]{2,1,0:T(8,128)}, u32[]{:S(2)}) copy-start(f32[16,16,64]{2,1,0:T(8,128)} %param.19) | copy-start | bytes 196612
  112.5 1.2 copy-start.8
  122.7 0.7 copy-start.6
where the time goes:
time: 125 us; the launch traced here: 124 us
  blocking collectives  76.3 us (61%)
  starting transfers between devices  13.7 us (11%)
  matrix products  13.5 us (11%)
  other arithmetic  9.79 us (8%)
  local copies, waits for them, and re-layouts  6.31 us (5%)
  waiting for transfers between devices  4.12 us (3%)
    all_gather x2, blocking collectives, gathered_once(): both, at, found = (lax.all_gather(jnp.concatenate(lines), axis), 0, {})  42.1 us
    all_to_all x2, blocking collectives, sent_to_all(): lax.all_to_all(jnp.broadcast_to(value[None], (peers, *value.shape)), axis...  34.2 us
    all_to_all x1, starting transfers between devices, on_device(): lax.all_to_all(normed, 'tp', split_axis=1, concat_axis=0, tiled=True)  13.7 us
    add x8, other arithmetic, prefix_states(): drive_im + rate_re * moved_im + rate_im * moved_re  6.78 us
    dot_general x1, matrix products, readout(): jnp.einsum('tgp,ghp->tgh', state_im, c_imag, precision=HIGHEST_PREC)  6.47 us
    dot_general x1, matrix products, readout(): first = jnp.einsum('tgp,ghp->tgh', state_re, c_real, precision=HIGHEST_PREC)  4.92 us
    all_to_all x1, waiting for transfers between devices, on_device(): lax.all_to_all(normed, 'tp', split_axis=1, concat_axis=0, tiled=True)  4.12 us
    unnamed x22, local copies, waits for them, and re-layouts  3.89 us
  transfers between devices with their start and end apart: 1, of which 1 were waited for; matrix products, arithmetic and copies ran while one was open for 0% of the time, Pallas kernels for 0%

commit v1 on v0

v1 whole, which is shorter than its diff:
```python
import functools

import jax
import jax.numpy as jnp
from jax import lax
from jax.experimental import pallas as pl
from jax.experimental.pallas import tpu as pltpu
from jax.sharding import Mesh
from jax.sharding import PartitionSpec as P

D = 2048
SP = ("sp_0", "sp_1")
SP_TP = ("sp_0", "sp_1", "tp")
NORM_EPS = 1e-06

F32 = jnp.float32
BF16 = jnp.bfloat16
ROWS = 192
TP = 8
STEPS = 24
WIDTH = 256
GROUPS = 16
STATE = 64
PAIRS = 8
LANES = 128
MESH = pl.DeviceIdType.MESH


def cmul(a, b):
    return (a[0] * b[0] - a[1] * b[1], a[0] * b[1] + a[1] * b[0])


def cmuladd(a, b, c):
    return (a[0] * b[0] - a[1] * b[1] + c[0], a[0] * b[1] + a[1] * b[0] + c[1])


def split_store(dst, g, real, imag):
    pair, second = g // 2, g % 2
    blank = jnp.zeros((16, STATE), F32)
    wide = [jnp.concatenate([blank, part] if second else [part, blank], axis=1) for part in (real, imag)]
    full = jnp.concatenate(wide, axis=1)
    high = full.astype(BF16)
    low = (full - high.astype(F32)).astype(BF16)
    row = 32 * (pair % 4) + 16 * second
    dst[pair, row : row + 16, :] = high
    dst[pair, LANES + row : LANES + row + 16, :] = low


def kernel(
    nz,
    ny,
    tok,
    nin,
    dl,
    ph,
    b_re,
    b_im,
    c_re,
    c_im,
    skip,
    wv,
    wg,
    nout,
    out,
    tok_v,
    nin_v,
    dl_v,
    ph_v,
    b_v,
    c_v,
    skip_v,
    wv_v,
    wg_v,
    nout_v,
    xs,
    xr,
    uf,
    wb,
    ct,
    dbuf,
    coef_v,
    wide_v,
    lam_v,
    pow_v,
    hop_v,
    fbuf,
    es,
    yr,
    zs,
    zr,
    held_v,
    sbuf,
    yv,
    zg,
    acc,
    gbuf,
    ss,
    sr,
    of,
    in_sem,
    xs_sem,
    xr_sem,
    ys_sem,
    yr_sem,
    zs_sem,
    zr_sem,
    gs_sem,
    gr_sem,
    qs_sem,
    qr_sem,
):
    me_z, me_y, me = lax.axis_index("sp_0"), lax.axis_index("sp_1"), lax.axis_index("tp")

    loads = []
    for k, (src, dst) in enumerate(
        (
            (tok, tok_v),
            (nin, nin_v),
            (dl, dl_v),
            (ph, ph_v),
            (b_re, b_v.at[0]),
            (b_im, b_v.at[1]),
            (c_re, c_v.at[0]),
            (c_im, c_v.at[1]),
            (skip, skip_v),
            (nout, nout_v),
            (wv, wv_v),
            (wg, wg_v),
        )
    ):
        load = pltpu.make_async_copy(src, dst, in_sem.at[k])
        load.start()
        loads.append(load)

    barrier = pltpu.get_barrier_semaphore()
    for k in range(1, nz):
        pl.semaphore_signal(barrier, inc=1, device_id={"sp_0": lax.rem(me_z + k, nz)}, device_id_type=MESH)
    for k in range(1, ny):
        pl.semaphore_signal(barrier, inc=1, device_id={"sp_1": lax.rem(me_y + k, ny)}, device_id_type=MESH)
    for k in range(1, TP):
        pl.semaphore_signal(barrier, inc=1, device_id={"tp": lax.rem(me + k, TP)}, device_id_type=MESH)

    loads[0].wait()
    loads[1].wait()
    x = tok_v[...].astype(F32)
    mean = jnp.sum(x * x, axis=1, keepdims=True) * (1.0 / D)
    normed = (x * lax.rsqrt(mean + NORM_EPS) * nin_v[...]).astype(BF16)
    for k in range(TP):
        xs[k] = normed[:, k * WIDTH : (k + 1) * WIDTH]

    loads[2].wait()
    loads[3].wait()
    decay, phase = dl_v[...], ph_v[...]
    magnitude = jnp.exp(decay)
    bar_re, bar_im = magnitude * jnp.cos(phase), magnitude * jnp.sin(phase)
    modulus = decay * decay + phase * phase
    coef_v[0] = ((bar_re - 1.0) * decay + bar_im * phase) / modulus
    coef_v[1] = (bar_im * decay - (bar_re - 1.0) * phase) / modulus
    wide_v[0] = jnp.concatenate([bar_re, bar_re], axis=1)
    wide_v[1] = jnp.concatenate([bar_im, bar_im], axis=1)
    left_half = lax.broadcasted_iota(jnp.int32, (PAIRS, LANES), 1) < STATE
    lam = tuple(
        jnp.where(left_half, wide_v[k, pl.ds(0, PAIRS, stride=2), :], wide_v[k, pl.ds(1, PAIRS, stride=2), :])
        for k in range(2)
    )
    lam2 = cmul(lam, lam)
    lam4 = cmul(lam2, lam2)
    lam8 = cmul(lam4, lam4)
    seg = cmul(cmul(lam8, lam8), lam8)
    lam_v[0], lam_v[1] = lam
    power = (jnp.ones((PAIRS, LANES), F32), jnp.zeros((PAIRS, LANES), F32))
    for j in range(TP):
        pow_v[0, j * PAIRS : (j + 1) * PAIRS, :], pow_v[1, j * PAIRS : (j + 1) * PAIRS, :] = power
        power = cmul(power, seg)
    hop = power
    power = (jnp.ones((PAIRS, LANES), F32), jnp.zeros((PAIRS, LANES), F32))
    for y in range(ny):
        hop_v[y, 0], hop_v[y, 1] = power
        power = cmul(power, hop)
    line = power
    loads[4].wait()
    loads[5].wait()
    wb[...] = jnp.zeros_like(wb)
    for g in range(GROUPS):
        split_store(wb, g, b_v[0, 16 * g : 16 * g + 16, :], b_v[1, 16 * g : 16 * g + 16, :])

    pl.semaphore_wait(barrier, nz + ny + TP - 3)

    xcopies = []
    for k in range(1, TP):
        peer = lax.rem(me + k, TP)
        copy = pltpu.make_async_remote_copy(
            xs.at[peer], xr.at[me], xs_sem.at[k - 1], xr_sem.at[k - 1], device_id={"tp": peer}, device_id_type=MESH
        )
        copy.start()
        xcopies.append(copy)
    xr[me] = xs[me]
    for k in range(1, TP):
        source = lax.rem(me + TP - k, TP)
        pltpu.make_async_remote_copy(
            xs.at[source], xr.at[source], xs_sem.at[k - 1], xr_sem.at[k - 1], device_id={"tp": source}, device_id_type=MESH
        ).wait_recv()

    for j in range(TP):
        block = xr[j].astype(F32)
        for q in range(2):
            uf[q, j * STEPS : (j + 1) * STEPS, :] = block[:, q * LANES : (q + 1) * LANES]
    for q in range(2):
        half = uf[q].astype(BF16)
        twice = jnp.concatenate([half, half], axis=1)
        for pair in range(4 * q, 4 * q + 4):
            drive = jnp.dot(twice, wb[pair], preferred_element_type=F32)
            dbuf[pair, 0] = drive[:, :LANES]
            dbuf[pair, 1] = drive[:, LANES:]

    def rate(pair):
        return tuple(jnp.broadcast_to(lam_v[k, pair : pair + 1, :], (TP, LANES)) for k in range(2))

    rates = [rate(pair) for pair in range(PAIRS)]

    def drive_at(pair, i):
        return (dbuf[pair, 0, pl.ds(i, TP, stride=STEPS), :], dbuf[pair, 1, pl.ds(i, TP, stride=STEPS), :])

    def first_pass(i, states):
        states = list(states)
        for sub in range(2):
            for pair in range(PAIRS):
                states[pair] = cmuladd(rates[pair], states[pair], drive_at(pair, 2 * i + sub))
        return tuple(states)

    nothing = jnp.zeros((TP, LANES), F32)
    ends = lax.fori_loop(0, STEPS // 2, first_pass, tuple((nothing, nothing) for _ in range(PAIRS)))
    segment = lax.broadcasted_iota(jnp.int32, (TP, LANES), 0)
    for pair in range(PAIRS):
        total = ends[pair]
        for shift in (1, 2, 4):
            moved = tuple(jnp.where(segment >= shift, pltpu.roll(part, shift, 0), 0.0) for part in total)
            decay_of = tuple(
                jnp.broadcast_to(pow_v[k, shift * PAIRS + pair : shift * PAIRS + pair + 1, :], (TP, LANES))
                for k in range(2)
            )
            total = cmuladd(decay_of, moved, total)
        for k in range(2):
            es[k, pair : pair + 1, :] = total[k][TP - 1 : TP, :]
            fbuf[pair, k] = jnp.where(segment >= 1, pltpu.roll(total[k], 1, 0), 0.0)

    ycopies = []
    for k in range(1, ny):
        peer = lax.rem(me_y + k, ny)
        copy = pltpu.make_async_remote_copy(
            es, yr.at[me_y], ys_sem.at[k - 1], yr_sem.at[k - 1], device_id={"sp_1": peer}, device_id_type=MESH
        )
        copy.start()
        ycopies.append(copy)
    yr[me_y] = es[...]

    loads[6].wait()
    loads[7].wait()
    ct[...] = jnp.zeros_like(ct)
    for g in range(GROUPS):
        own = (c_v[0, 16 * g : 16 * g + 16, :], c_v[1, 16 * g : 16 * g + 16, :])
        real, imag = cmul(own, (coef_v[0, g : g + 1, :], coef_v[1, g : g + 1, :]))
        split_store(ct, g, real, -imag)

    for k in range(1, ny):
        source = lax.rem(me_y + ny - k, ny)
        pltpu.make_async_remote_copy(
            es, yr.at[source], ys_sem.at[k - 1], yr_sem.at[k - 1], device_id={"sp_1": source}, device_id_type=MESH
        ).wait_recv()
    empty = (jnp.zeros((PAIRS, LANES), F32), jnp.zeros((PAIRS, LANES), F32))
    total, inside = empty, empty
    for y in range(ny):
        inside = tuple(jnp.where(me_y == y, new, old) for new, old in zip(total, inside))
        total = cmuladd(hop, total, (yr[y, 0], yr[y, 1]))
    zs[0], zs[1] = total

    def zcopy(k, peer, slot):
        return pltpu.make_async_remote_copy(
            zs, zr.at[slot], zs_sem.at[k - 1], zr_sem.at[k - 1], device_id={"sp_0": peer}, device_id_type=MESH
        )

    for k in range(1, nz):

        @pl.when(me_z + k < nz)
        def _(k=k):
            zcopy(k, me_z + k, me_z).start()

    held_v[...] = jnp.zeros_like(held_v)
    for k in range(nz - 1, 0, -1):

        @pl.when(me_z >= k)
        def _(k=k):
            zcopy(k, me_z - k, me_z - k).wait_recv()
            new = cmuladd(line, (held_v[0], held_v[1]), (zr[me_z - k, 0], zr[me_z - k, 1]))
            held_v[0], held_v[1] = new

    held = cmuladd((hop_v[me_y, 0], hop_v[me_y, 1]), (held_v[0], held_v[1]), inside)
    held_v[0], held_v[1] = held

    starts = []
    for pair in range(PAIRS):
        carried = tuple(jnp.broadcast_to(held_v[k, pair : pair + 1, :], (TP, LANES)) for k in range(2))
        reach = tuple(pow_v[k, pl.ds(pair, TP, stride=PAIRS), :] for k in range(2))
        starts.append(cmuladd(reach, carried, (fbuf[pair, 0], fbuf[pair, 1])))

    def second_pass(i, states):
        states = list(states)
        row = pl.multiple_of(2 * TP * i, 2 * TP)
        for pair in range(PAIRS):
            one = cmuladd(rates[pair], states[pair], drive_at(pair, 2 * i))
            two = cmuladd(rates[pair], one, drive_at(pair, 2 * i + 1))
            for k in range(2):
                both = jnp.concatenate([one[k], two[k]], axis=0).astype(BF16)
                sbuf[pair, pl.ds(row, 2 * TP), k * LANES : (k + 1) * LANES] = both
            states[pair] = two
        return tuple(states)

    lax.fori_loop(0, STEPS // 2, second_pass, tuple(starts))

    loads[8].wait()
    for q in range(2):
        both = None
        for pair in range(4 * q, 4 * q + 4):
            part = lax.dot_general(sbuf[pair], ct[pair], (((1,), (1,)), ((), ())), preferred_element_type=F32)
            both = part if both is None else both + part
        yv[q] = both[:, :LANES] + both[:, LANES:]

    def activate(i, _):
        row = pl.multiple_of(2 * TP * i, 2 * TP)
        for q in range(2):
            gain = skip_v[:, q * LANES : (q + 1) * LANES]
            direct = jnp.concatenate([uf[q, pl.ds(2 * i + sub, TP, stride=STEPS), :] for sub in range(2)], axis=0)
            pre = yv[q, pl.ds(row, 2 * TP), :] + gain * direct
            z = jax.nn.gelu(pre)
            zg[me, pl.ds(row, 2 * TP), q * LANES : (q + 1) * LANES] = z.astype(BF16)
        return 0

    lax.fori_loop(0, STEPS // 2, activate, 0)

    chip, core = lax.div(me, 2), lax.rem(me, 2)
    partner = me + 1 - 2 * core
    right = lax.rem(chip + 1, TP // 2) * 2 + core
    left = lax.rem(chip + TP // 2 - 1, TP // 2) * 2 + core
    far = lax.rem(chip + 2, TP // 2) * 2 + core
    other = 1 - 2 * core

    def gcopy(n, owner, half, peer):
        part = zg.at[owner, pl.ds(half * (ROWS // 2), ROWS // 2), :]
        return pltpu.make_async_remote_copy(
            part, part, gs_sem.at[n], gr_sem.at[n], device_id={"tp": peer}, device_id_type=MESH
        )

    def send(n, owner, half, peer):
        gcopy(n, owner, half, peer).start()

    def arrived(n, owner, half, peer):
        gcopy(n, owner, half, peer).wait_recv()

    for half in range(2):
        send(half, me, half, right)
        send(2 + half, me, half, left)
        send(4 + half, me, half, partner)

    def project(owner, first=False):
        rows = pl.ds(pl.multiple_of(owner * WIDTH, WIDTH), WIDTH)
        block = zg[owner]
        for k, weight in enumerate((wv_v, wg_v)):
            part = jnp.dot(block, weight[rows, :], preferred_element_type=F32)
            if first:
                acc[k] = part
            else:
                acc[k] += part

    loads[10].wait()
    loads[11].wait()
    project(me, first=True)
    arrived(0, left, 0, left)
    send(6, left, 0, right)
    send(8, left, 0, partner)
    arrived(2, right, 0, right)
    send(10, right, 0, partner)
    arrived(4, partner, 0, partner)
    arrived(5, partner, 1, partner)
    project(partner)
    arrived(3, right, 1, right)
    send(7, right, 1, left)
    send(11, right, 1, partner)
    arrived(1, left, 1, left)
    send(9, left, 1, partner)
    project(right)
    project(left)
    arrived(6, far, 0, left)
    send(12, far, 0, partner)
    arrived(7, far, 1, right)
    send(13, far, 1, partner)
    for half in range(2):
        arrived(8 + half, left + other, half, partner)
    project(left + other)
    for half in range(2):
        arrived(10 + half, right + other, half, partner)
    project(right + other)
    project(far)
    for half in range(2):
        arrived(12 + half, far + other, half, partner)
    project(far + other)

    ss[...] = jnp.zeros_like(ss)
    lane = lax.broadcasted_iota(jnp.int32, (TP, LANES), 1)

    def gate(i, _):
        rows = pl.ds(pl.multiple_of(TP * i, TP), TP)
        gated = acc[0, rows, :] * jax.nn.sigmoid(acc[1, rows, :])
        gbuf[rows, :] = gated
        own = jnp.sum(gated * gated, axis=1, keepdims=True)
        ss[...] = jnp.where(lane == i, own, ss[...])
        return 0

    lax.fori_loop(0, STEPS, gate, 0)
    qcopies = []
    for k in range(1, TP):
        peer = lax.rem(me + k, TP)
        copy = pltpu.make_async_remote_copy(
            ss, sr.at[me], qs_sem.at[k - 1], qr_sem.at[k - 1], device_id={"tp": peer}, device_id_type=MESH
        )
        copy.start()
        qcopies.append(copy)
    sr[me] = ss[...]
    loads[9].wait()
    for k in range(1, TP):
        source = lax.rem(me + TP - k, TP)
        pltpu.make_async_remote_copy(
            ss, sr.at[source], qs_sem.at[k - 1], qr_sem.at[k - 1], device_id={"tp": source}, device_id_type=MESH
        ).wait_recv()
    squares = sr[0]
    for k in range(1, TP):
        squares = squares + sr[k]
    scale = lax.rsqrt(squares * (1.0 / D) + NORM_EPS)
    for i in range(STEPS):
        done = gbuf[i * TP : (i + 1) * TP, :] * scale[:, i : i + 1] * nout_v[...]
        for q in range(2):
            of[q, pl.ds(i, TP, stride=STEPS), :] = done[:, q * LANES : (q + 1) * LANES]
    for q in range(2):
        out[:, q * LANES : (q + 1) * LANES] = of[q].astype(BF16)

    for copy in xcopies + ycopies + qcopies:
        copy.wait_send()
    for k in range(1, nz):

        @pl.when(me_z + k < nz)
        def _(k=k):
            zcopy(k, me_z + k, me_z).wait_send()

    for n in range(14):
        gcopy(n, me, 0, partner).wait_send()


def on_device(nz, ny, tokens, norm_in, decay_log, phase, b_real, b_imag, c_real, c_imag, skip_gain, w_value, w_gate, norm_out):
    def by_channel(b):
        return b.transpose(0, 2, 1).reshape(WIDTH, STATE)

    dma = pltpu.SemaphoreType.DMA
    scratch = [
        pltpu.VMEM((STEPS, D), BF16),
        pltpu.VMEM((1, D), F32),
        pltpu.VMEM((GROUPS, STATE), F32),
        pltpu.VMEM((GROUPS, STATE), F32),
        pltpu.VMEM((2, WIDTH, STATE), F32),
        pltpu.VMEM((2, WIDTH, STATE), F32),
        pltpu.VMEM((1, WIDTH), F32),
        pltpu.VMEM((D, WIDTH), BF16),
        pltpu.VMEM((D, WIDTH), BF16),
        pltpu.VMEM((1, WIDTH), F32),
        pltpu.VMEM((TP, STEPS, WIDTH), BF16),
        pltpu.VMEM((TP, STEPS, WIDTH), BF16),
        pltpu.VMEM((2, ROWS, LANES), F32),
        pltpu.VMEM((PAIRS, 2 * LANES, 2 * LANES), BF16),
        pltpu.VMEM((PAIRS, 2 * LANES, 2 * LANES), BF16),
        pltpu.VMEM((PAIRS, 2, ROWS, LANES), F32),
        pltpu.VMEM((2, GROUPS, STATE), F32),
        pltpu.VMEM((2, GROUPS, LANES), F32),
        pltpu.VMEM((2, PAIRS, LANES), F32),
        pltpu.VMEM((2, TP * PAIRS, LANES), F32),
        pltpu.VMEM((ny, 2, PAIRS, LANES), F32),
        pltpu.VMEM((PAIRS, 2, TP, LANES), F32),
        pltpu.VMEM((2, PAIRS, LANES), F32),
        pltpu.VMEM((ny, 2, PAIRS, LANES), F32),
        pltpu.VMEM((2, PAIRS, LANES), F32),
        pltpu.VMEM((nz, 2, PAIRS, LANES), F32),
        pltpu.VMEM((2, PAIRS, LANES), F32),
        pltpu.VMEM((PAIRS, ROWS, 2 * LANES), BF16),
        pltpu.VMEM((2, ROWS, LANES), F32),
        pltpu.VMEM((TP, ROWS, WIDTH), BF16),
        pltpu.VMEM((2, ROWS, WIDTH), F32),
        pltpu.VMEM((ROWS, WIDTH), F32),
        pltpu.VMEM((TP, LANES), F32),
        pltpu.VMEM((TP, TP, LANES), F32),
        pltpu.VMEM((2, ROWS, LANES), F32),
        dma((12,)),
        dma((TP - 1,)),
        dma((TP - 1,)),
        dma((ny - 1,)),
        dma((ny - 1,)),
        dma((nz - 1,)),
        dma((nz - 1,)),
        dma((14,)),
        dma((14,)),
        dma((TP - 1,)),
        dma((TP - 1,)),
    ]
    return pl.pallas_call(
        functools.partial(kernel, nz, ny),
        out_shape=jax.ShapeDtypeStruct((ROWS, WIDTH), BF16),
        in_specs=[pl.BlockSpec(memory_space=pl.ANY)] * 12,
        out_specs=pl.BlockSpec(memory_space=pltpu.VMEM),
        scratch_shapes=scratch,
        compiler_params=pltpu.CompilerParams(
            collective_id=0, has_side_effects=True, vmem_limit_bytes=48 * 1024 * 1024
        ),
        name="mixer",
    )(
        tokens,
        norm_in.reshape(1, D),
        decay_log,
        phase,
        by_channel(b_real),
        by_channel(b_imag),
        c_real.reshape(WIDTH, STATE),
        c_imag.reshape(WIDTH, STATE),
        skip_gain.reshape(1, WIDTH),
        w_value,
        w_gate,
        norm_out.reshape(1, WIDTH),
    )


def solution(mesh):
    torus = Mesh(mesh.devices.reshape(-1, 8, mesh.shape["tp"]), SP_TP)
    return on_torus(torus)


def on_torus(torus):
    in_specs = (
        P(SP_TP, None),
        P(),
        P("tp", None),
        P("tp", None),
        P("tp", None, None),
        P("tp", None, None),
        P("tp", None, None),
        P("tp", None, None),
        P("tp"),
        P(None, "tp"),
        P(None, "tp"),
        P("tp"),
    )
    return jax.shard_map(
        functools.partial(on_device, torus.shape["sp_0"], torus.shape["sp_1"]),
        mesh=torus,
        in_specs=in_specs,
        out_specs=P(SP, "tp"),
        check_vma=False,
    )
```

time: 125 us -> 58 us (0.46)
  the two profiles are of different devices: /device:TPU:1 before, /device:TPU:65 now
where the time goes in v1:
time: 58 us; the launch traced here: 57.5 us
  Pallas kernels  47.8 us (82%)
  local copies, waits for them, and re-layouts  9.7 us (17%)
    pallas_call x1, Pallas kernels, on_device(): pl.pallas_call(functools.partial(kernel, nz, ny), out_shape=jax.ShapeDtyp...  47.8 us
    unnamed x25, local copies, waits for them, and re-layouts  9.7 us

profile of v1, /device:TPU:65, one launch (start us, length us, event | category | flops | bytes accessed | tf_op | source)
XLA Modules:
  0.0 57.5 jit_solution(9072945921842914368)
XLA Ops:
  0.0 0.0 copy-start.7
  0.0 0.0 copy-start.11
  0.0 0.0 copy-start.10
  0.0 0.7 %copy-done.7 = f32[2048]{0:T(1024)S(1)} copy-done((f32[2048]{0:T(1024)S(1)}, f32[2048]{0:T(1024)}, u32[]{:S(2)}) %copy-start.7) | copy-done | bytes 8216
  0.7 0.0 copy-done.11
  0.7 0.0 copy-done.10
  0.7 0.0 copy-start
  0.7 1.2 %copy-done = bf16[2048,256]{1,0:T(8,128)(2,1)S(1)} copy-done((bf16[2048,256]{1,0:T(8,128)(2,1)S(1)}, bf16[2048,256]{1,0:T(8,128)(2,1)}, u32[]{:S(2)}) %copy-start) | copy-done | bytes 1048600
  1.9 0.0 copy-start.1
  1.9 1.2 %copy-done.1 = bf16[2048,256]{1,0:T(8,128)(2,1)S(1)} copy-done((bf16[2048,256]{1,0:T(8,128)(2,1)S(1)}, bf16[2048,256]{1,0:T(8,128)(2,1)}, u32[]{:S(2)}) %copy-start.1) | copy-done | bytes 1048600
  3.2 0.0 copy-start.2
  3.2 0.9 %copy-done.2 = f32[16,64,16]{1,2,0:T(8,128)S(1)} copy-done((f32[16,64,16]{1,2,0:T(8,128)S(1)}, f32[16,64,16]{1,2,0:T(8,128)}, u32[]{:S(2)}) %copy-start.2) | copy-done | bytes 65560
  4.1 0.0 copy-start.3
  4.1 0.9 %copy-done.3 = f32[16,64,16]{1,2,0:T(8,128)S(1)} copy-done((f32[16,64,16]{1,2,0:T(8,128)S(1)}, f32[16,64,16]{1,2,0:T(8,128)}, u32[]{:S(2)}) %copy-start.3) | copy-done | bytes 65560
  5.0 0.0 copy-start.4
  5.0 0.9 %copy-done.4 = f32[16,16,64]{2,1,0:T(8,128)S(1)} copy-done((f32[16,16,64]{2,1,0:T(8,128)S(1)}, f32[16,16,64]{2,1,0:T(8,128)}, u32[]{:S(2)}) %copy-start.4) | copy-done | bytes 65560
  5.9 0.0 copy-start.5
  5.9 0.9 %copy-done.5 = f32[16,16,64]{2,1,0:T(8,128)S(1)} copy-done((f32[16,16,64]{2,1,0:T(8,128)S(1)}, f32[16,16,64]{2,1,0:T(8,128)}, u32[]{:S(2)}) %copy-start.5) | copy-done | bytes 65560
  6.8 0.0 copy-start.6
  6.8 0.9 %copy-done.6 = bf16[24,2048]{1,0:T(8,128)(2,1)S(1)} copy-done((bf16[24,2048]{1,0:T(8,128)(2,1)S(1)}, bf16[24,2048]{1,0:T(8,128)(2,1)}, u32[]{:S(2)}) %copy-start.6) | copy-done | bytes 98328
  7.7 0.0 copy-start.8
  7.7 0.7 %copy-done.8 = f32[16,64]{1,0:T(8,128)S(1)} copy-done((f32[16,64]{1,0:T(8,128)S(1)}, f32[16,64]{1,0:T(8,128)}, u32[]{:S(2)}) %copy-start.8) | copy-done | bytes 4120
  8.4 0.0 copy-start.9
  8.4 0.7 %copy-done.9 = f32[16,64]{1,0:T(8,128)S(1)} copy-done((f32[16,64]{1,0:T(8,128)S(1)}, f32[16,64]{1,0:T(8,128)}, u32[]{:S(2)}) %copy-start.9) | copy-done | bytes 4120
  9.1 47.8 %mixer.1 = bf16[192,256]{1,0:T(8,128)(2,1)S(1)} custom-call(bf16[24,2048]{1,0:T(8,128)(2,1)S(1)} %copy-done.6, f32[1,2048]{1,0:T(1,128)S(1)} %bitcast.15, f32[16,64]{1,0:T(8,128)S(1)} %copy-done.8, f32[16,64]{1,0:T(8,128)S(1)} %copy-done.9, f32[256,64]{1,0:T(8,128)S(1)} %bitcast.11, f32[256,64]{1,0:T(8,128)S(1)} %bitcast.12, f32[256,64]{1,0:T(8,128)S(1)} %bitcast.13, ...), custom_call_target="tpu_custom_call" | custom-call | tf_op jit(solution)/shard_map/mixer/pallas_call | solution.py:510
  56.9 0.6 %copy.14 = bf16[192,256]{1,0:T(8,128)(2,1)} copy(bf16[192,256]{1,0:T(8,128)(2,1)S(1)} %mixer.1) | data formatting | bytes 196608
Async XLA Ops:
  0.0 0.7 %copy-start.7 = (f32[2048]{0:T(1024)S(1)}, f32[2048]{0:T(1024)}, u32[]{:S(2)}) copy-start(f32[2048]{0:T(1024)} %param.13) | copy-start | bytes 24580
  0.0 0.7 %copy-start.11 = (f32[256]{0:T(256)S(1)}, f32[256]{0:T(256)}, u32[]{:S(2)}) copy-start(f32[256]{0:T(256)} %param.23) | copy-start | bytes 3076
  0.0 0.7 %copy-start.10 = (f32[256]{0:T(256)S(1)}, f32[256]{0:T(256)}, u32[]{:S(2)}) copy-start(f32[256]{0:T(256)} %param.20) | copy-start | bytes 3076
  0.7 1.2 %copy-start = (bf16[2048,256]{1,0:T(8,128)(2,1)S(1)}, bf16[2048,256]{1,0:T(8,128)(2,1)}, u32[]{:S(2)}) copy-start(bf16[2048,256]{1,0:T(8,128)(2,1)} %wv.1) | copy-start | bytes 3145732
  1.9 1.2 %copy-start.1 = (bf16[2048,256]{1,0:T(8,128)(2,1)S(1)}, bf16[2048,256]{1,0:T(8,128)(2,1)}, u32[]{:S(2)}) copy-start(bf16[2048,256]{1,0:T(8,128)(2,1)} %wg.1) | copy-start | bytes 3145732
  3.2 0.9 %copy-start.2 = (f32[16,64,16]{1,2,0:T(8,128)S(1)}, f32[16,64,16]{1,2,0:T(8,128)}, u32[]{:S(2)}) copy-start(f32[16,64,16]{1,2,0:T(8,128)} %param.16) | copy-start | bytes 196612
  4.1 0.9 %copy-start.3 = (f32[16,64,16]{1,2,0:T(8,128)S(1)}, f32[16,64,16]{1,2,0:T(8,128)}, u32[]{:S(2)}) copy-start(f32[16,64,16]{1,2,0:T(8,128)} %param.17) | copy-start | bytes 196612
  5.0 0.9 %copy-start.4 = (f32[16,16,64]{2,1,0:T(8,128)S(1)}, f32[16,16,64]{2,1,0:T(8,128)}, u32[]{:S(2)}) copy-start(f32[16,16,64]{2,1,0:T(8,128)} %param.18) | copy-start | bytes 196612
  5.9 0.9 %copy-start.5 = (f32[16,16,64]{2,1,0:T(8,128)S(1)}, f32[16,16,64]{2,1,0:T(8,128)}, u32[]{:S(2)}) copy-start(f32[16,16,64]{2,1,0:T(8,128)} %param.19) | copy-start | bytes 196612
  6.8 0.9 %copy-start.6 = (bf16[24,2048]{1,0:T(8,128)(2,1)S(1)}, bf16[24,2048]{1,0:T(8,128)(2,1)}, u32[]{:S(2)}) copy-start(bf16[24,2048]{1,0:T(8,128)(2,1)} %tok.1) | copy-start | bytes 294916
  7.7 0.7 %copy-start.8 = (f32[16,64]{1,0:T(8,128)S(1)}, f32[16,64]{1,0:T(8,128)}, u32[]{:S(2)}) copy-start(f32[16,64]{1,0:T(8,128)} %dl.1) | copy-start | bytes 12292
  8.4 0.7 %copy-start.9 = (f32[16,64]{1,0:T(8,128)S(1)}, f32[16,64]{1,0:T(8,128)}, u32[]{:S(2)}) copy-start(f32[16,64]{1,0:T(8,128)} %ph.1) | copy-start | bytes 12292

commit v2 on v1

--- a/solution.py
+++ b/solution.py
@@ -23,6 +23,9 @@
 STATE = 64
 PAIRS = 8
 LANES = 128
+CHAIN = 4
+FAR_FIRST = (4, 3, 5, 2, 6, 1, 7)
+CHUNKS = 4
 MESH = pl.DeviceIdType.MESH
 
 
@@ -104,41 +107,66 @@
     yr_sem,
     zs_sem,
     zr_sem,
+    here_sem,
     gs_sem,
     gr_sem,
+    ps_sem,
+    pr_sem,
     qs_sem,
     qr_sem,
 ):
     me_z, me_y, me = lax.axis_index("sp_0"), lax.axis_index("sp_1"), lax.axis_index("tp")
-
-    loads = []
-    for k, (src, dst) in enumerate(
-        (
-            (tok, tok_v),
-            (nin, nin_v),
-            (dl, dl_v),
-            (ph, ph_v),
-            (b_re, b_v.at[0]),
-            (b_im, b_v.at[1]),
-            (c_re, c_v.at[0]),
-            (c_im, c_v.at[1]),
-            (skip, skip_v),
-            (nout, nout_v),
-            (wv, wv_v),
-            (wg, wg_v),
-        )
-    ):
-        load = pltpu.make_async_copy(src, dst, in_sem.at[k])
+    y_order = [k for k in FAR_FIRST if k < ny]
+    reach = min(CHAIN, nz - 1)
+
+    loads = [
+        pltpu.make_async_copy(src, dst, in_sem.at[k])
+        for k, (src, dst) in enumerate(
+            (
+                (tok, tok_v),
+                (nin, nin_v),
+                (dl, dl_v),
+                (ph, ph_v),
+                (b_re, b_v.at[0]),
+                (b_im, b_v.at[1]),
+                (c_re, c_v.at[0]),
+                (c_im, c_v.at[1]),
+                (skip, skip_v),
+                (nout, nout_v),
+                (wv, wv_v),
+                (wg, wg_v),
+            )
+        )
+    ]
+    for load in loads[:4]:
         load.start()
-        loads.append(load)
 
     barrier = pltpu.get_barrier_semaphore()
-    for k in range(1, nz):
-        pl.semaphore_signal(barrier, inc=1, device_id={"sp_0": lax.rem(me_z + k, nz)}, device_id_type=MESH)
-    for k in range(1, ny):
+    for k in FAR_FIRST:
+        pl.semaphore_signal(barrier, inc=1, device_id={"tp": lax.rem(me + k, TP)}, device_id_type=MESH)
+    for k in y_order:
         pl.semaphore_signal(barrier, inc=1, device_id={"sp_1": lax.rem(me_y + k, ny)}, device_id_type=MESH)
-    for k in range(1, TP):
-        pl.semaphore_signal(barrier, inc=1, device_id={"tp": lax.rem(me + k, TP)}, device_id_type=MESH)
+
+    @pl.when(me_z > 0)
+    def _():
+        pl.semaphore_signal(barrier, inc=1, device_id={"sp_0": me_z - 1}, device_id_type=MESH)
+
+    @pl.when(me_z + 1 < nz)
+    def _():
+        pl.semaphore_signal(barrier, inc=1, device_id={"sp_0": me_z + 1}, device_id_type=MESH)
+
+    for load in loads[4:]:
+        load.start()
+
+    def tell(r):
+        @pl.when((me_z > 0) & (me_z + r < nz))
+        def _():
+            pl.semaphore_signal(here_sem.at[r - 1], inc=1, device_id={"sp_0": me_z - 1}, device_id_type=MESH)
+
+    def hear(r):
+        @pl.when(me_z + 1 + r < nz)
+        def _():
+            pl.semaphore_wait(here_sem.at[r - 1], 1)
 
     loads[0].wait()
     loads[1].wait()
@@ -184,10 +212,12 @@
     for g in range(GROUPS):
         split_store(wb, g, b_v[0, 16 * g : 16 * g + 16, :], b_v[1, 16 * g : 16 * g + 16, :])
 
-    pl.semaphore_wait(barrier, nz + ny + TP - 3)
+    neighbours = jnp.minimum(me_z, 1) + jnp.minimum(nz - 1 - me_z, 1)
+    pl.semaphore_wait(barrier, ny + TP - 2 + neighbours)
+    tell(1)
 
     xcopies = []
-    for k in range(1, TP):
+    for k in FAR_FIRST:
         peer = lax.rem(me + k, TP)
         copy = pltpu.make_async_remote_copy(
             xs.at[peer], xr.at[me], xs_sem.at[k - 1], xr_sem.at[k - 1], device_id={"tp": peer}, device_id_type=MESH
@@ -200,6 +230,10 @@
         pltpu.make_async_remote_copy(
             xs.at[source], xr.at[source], xs_sem.at[k - 1], xr_sem.at[k - 1], device_id={"tp": source}, device_id_type=MESH
         ).wait_recv()
+
+    if reach > 1:
+        hear(1)
+        tell(2)
 
     for j in range(TP):
         block = xr[j].astype(F32)
@@ -245,7 +279,7 @@
             fbuf[pair, k] = jnp.where(segment >= 1, pltpu.roll(total[k], 1, 0), 0.0)
 
     ycopies = []
-    for k in range(1, ny):
+    for k in y_order:
         peer = lax.rem(me_y + k, ny)
         copy = pltpu.make_async_remote_copy(
             es, yr.at[me_y], ys_sem.at[k - 1], yr_sem.at[k - 1], device_id={"sp_1": peer}, device_id_type=MESH
@@ -272,36 +306,49 @@
     for y in range(ny):
         inside = tuple(jnp.where(me_y == y, new, old) for new, old in zip(total, inside))
         total = cmuladd(hop, total, (yr[y, 0], yr[y, 1]))
-    zs[0], zs[1] = total
-
-    def zcopy(k, peer, slot):
+    zs[0, 0], zs[0, 1] = total
+    def zcopy(k, peer):
         return pltpu.make_async_remote_copy(
-            zs, zr.at[slot], zs_sem.at[k - 1], zr_sem.at[k - 1], device_id={"sp_0": peer}, device_id_type=MESH
-        )
-
-    for k in range(1, nz):
-
+            zs.at[k // CHAIN],
+            zr.at[k - 1],
+            zs_sem.at[k - 1],
+            zr_sem.at[k - 1],
+            device_id={"sp_0": peer},
+            device_id_type=MESH,
+        )
+
+    def zsend(k):
         @pl.when(me_z + k < nz)
-        def _(k=k):
-            zcopy(k, me_z + k, me_z).start()
-
+        def _():
+            zcopy(k, me_z + k).start()
+
+    zsend(1)
+    for k in range(2, min(reach, CHAIN - 1) + 1):
+        if k > 2:
+            hear(k - 1)
+            tell(k)
+        zsend(k)
     held_v[...] = jnp.zeros_like(held_v)
-    for k in range(nz - 1, 0, -1):
+    for k in range(reach, 0, -1):
 
         @pl.when(me_z >= k)
         def _(k=k):
-            zcopy(k, me_z - k, me_z - k).wait_recv()
-            new = cmuladd(line, (held_v[0], held_v[1]), (zr[me_z - k, 0], zr[me_z - k, 1]))
+            zcopy(k, me_z - k).wait_recv()
+            new = cmuladd(line, (held_v[0], held_v[1]), (zr[k - 1, 0], zr[k - 1, 1]))
             held_v[0], held_v[1] = new
 
+    if reach == CHAIN:
+        zs[1, 0], zs[1, 1] = cmuladd(line, (held_v[0], held_v[1]), total)
+        hear(CHAIN - 1)
+        zsend(CHAIN)
     held = cmuladd((hop_v[me_y, 0], hop_v[me_y, 1]), (held_v[0], held_v[1]), inside)
     held_v[0], held_v[1] = held
 
     starts = []
     for pair in range(PAIRS):
         carried = tuple(jnp.broadcast_to(held_v[k, pair : pair + 1, :], (TP, LANES)) for k in range(2))
-        reach = tuple(pow_v[k, pl.ds(pair, TP, stride=PAIRS), :] for k in range(2))
-        starts.append(cmuladd(reach, carried, (fbuf[pair, 0], fbuf[pair, 1])))
+        since = tuple(pow_v[k, pl.ds(pair, TP, stride=PAIRS), :] for k in range(2))
+        starts.append(cmuladd(since, carried, (fbuf[pair, 0], fbuf[pair, 1])))
 
     def second_pass(i, states):
         states = list(states)
@@ -344,22 +391,20 @@
     far = lax.rem(chip + 2, TP // 2) * 2 + core
     other = 1 - 2 * core
 
-    def gcopy(n, owner, half, peer):
-        part = zg.at[owner, pl.ds(half * (ROWS // 2), ROWS // 2), :]
+    def rows_of(owner, chunk, count):
+        return zg.at[owner, pl.ds(chunk * (ROWS // CHUNKS), count * (ROWS // CHUNKS)), :]
+
+    def gcopy(n, owner, chunk, peer):
+        part = rows_of(owner, chunk, 1)
         return pltpu.make_async_remote_copy(
             part, part, gs_sem.at[n], gr_sem.at[n], device_id={"tp": peer}, device_id_type=MESH
         )
 
-    def send(n, owner, half, peer):
-        gcopy(n, owner, half, peer).start()
-
-    def arrived(n, owner, half, peer):
-        gcopy(n, owner, half, peer).wait_recv()
-
-    for half in range(2):
-        send(half, me, half, right)
-        send(2 + half, me, half, left)
-        send(4 + half, me, half, partner)
+    def pcopy(n, owner, chunk, count):
+        part = rows_of(owner, chunk, count)
+        return pltpu.make_async_remote_copy(
+            part, part, ps_sem.at[n], pr_sem.at[n], device_id={"tp": partner}, device_id_type=MESH
+        )
 
     def project(owner, first=False):
         rows = pl.ds(pl.multiple_of(owner * WIDTH, WIDTH), WIDTH)
@@ -371,53 +416,58 @@
             else:
                 acc[k] += part
 
+    right_order, left_order = (0, 1, 2, 3), (2, 3, 0, 1)
+    for k in range(CHUNKS):
+        gcopy(right_order[k], me, right_order[k], right).start()
+        gcopy(4 + left_order[k], me, left_order[k], left).start()
+        if k == 0:
+            pcopy(0, me, 0, CHUNKS).start()
+
     loads[10].wait()
     loads[11].wait()
     project(me, first=True)
-    arrived(0, left, 0, left)
-    send(6, left, 0, right)
-    send(8, left, 0, partner)
-    arrived(2, right, 0, right)
-    send(10, right, 0, partner)
-    arrived(4, partner, 0, partner)
-    arrived(5, partner, 1, partner)
+    pcopy(0, partner, 0, CHUNKS).wait_recv()
     project(partner)
-    arrived(3, right, 1, right)
-    send(7, right, 1, left)
-    send(11, right, 1, partner)
-    arrived(1, left, 1, left)
-    send(9, left, 1, partner)
+    for k in range(2):
+        gcopy(k, left, k, left).wait_recv()
+        gcopy(8 + k, left, k, right).start()
+        gcopy(4 + 2 + k, right, 2 + k, right).wait_recv()
+        gcopy(8 + 2 + k, right, 2 + k, left).start()
+    pcopy(1, left, 0, 2).start()
+    pcopy(2, right, 2, 2).start()
+    for k in range(2):
+        gcopy(2 + k, left, 2 + k, left).wait_recv()
+        gcopy(4 + k, right, k, right).wait_recv()
+    pcopy(3, left, 2, 2).start()
+    pcopy(4, right, 0, 2).start()
+    project(left)
     project(right)
-    project(left)
-    arrived(6, far, 0, left)
-    send(12, far, 0, partner)
-    arrived(7, far, 1, right)
-    send(13, far, 1, partner)
-    for half in range(2):
-        arrived(8 + half, left + other, half, partner)
+    for k in range(2):
+        gcopy(8 + k, far, k, left).wait_recv()
+        gcopy(12 + k, far, k, partner).start()
+        gcopy(8 + 2 + k, far, 2 + k, right).wait_recv()
+        gcopy(12 + 2 + k, far, 2 + k, partner).start()
+    pcopy(1, left + other, 0, 2).wait_recv()
+    pcopy(3, left + other, 2, 2).wait_recv()
     project(left + other)
-    for half in range(2):
-        arrived(10 + half, right + other, half, partner)
+    pcopy(2, right + other, 2, 2).wait_recv()
+    pcopy(4, right + other, 0, 2).wait_recv()
     project(right + other)
     project(far)
-    for half in range(2):
-        arrived(12 + half, far + other, half, partner)
+    for k in range(CHUNKS):
+        gcopy(12 + k, far + other, k, partner).wait_recv()
     project(far + other)
 
-    ss[...] = jnp.zeros_like(ss)
     lane = lax.broadcasted_iota(jnp.int32, (TP, LANES), 1)
-
-    def gate(i, _):
-        rows = pl.ds(pl.multiple_of(TP * i, TP), TP)
+    sums = jnp.zeros((TP, LANES), F32)
+    for i in range(STEPS):
+        rows = slice(TP * i, TP * i + TP)
         gated = acc[0, rows, :] * jax.nn.sigmoid(acc[1, rows, :])
         gbuf[rows, :] = gated
-        own = jnp.sum(gated * gated, axis=1, keepdims=True)
-        ss[...] = jnp.where(lane == i, own, ss[...])
-        return 0
-
-    lax.fori_loop(0, STEPS, gate, 0)
+        sums = jnp.where(lane == i, jnp.sum(gated * gated, axis=1, keepdims=True), sums)
+    ss[...] = sums
     qcopies = []
-    for k in range(1, TP):
+    for k in FAR_FIRST:
         peer = lax.rem(me + k, TP)
         copy = pltpu.make_async_remote_copy(
             ss, sr.at[me], qs_sem.at[k - 1], qr_sem.at[k - 1], device_id={"tp": peer}, device_id_type=MESH
@@ -444,14 +494,17 @@
 
     for copy in xcopies + ycopies + qcopies:
         copy.wait_send()
-    for k in range(1, nz):
+    for k in range(1, reach + 1):
 
         @pl.when(me_z + k < nz)
         def _(k=k):
-            zcopy(k, me_z + k, me_z).wait_send()
-
-    for n in range(14):
+            zcopy(k, me_z + k).wait_send()
+
+    for n in range(16):
         gcopy(n, me, 0, partner).wait_send()
+    pcopy(0, me, 0, CHUNKS).wait_send()
+    for n in range(1, 5):
+        pcopy(n, me, 0, 2).wait_send()
 
 
 def on_device(nz, ny, tokens, norm_in, decay_log, phase, b_real, b_imag, c_real, c_imag, skip_gain, w_value, w_gate, norm_out):
@@ -484,8 +537,8 @@
         pltpu.VMEM((PAIRS, 2, TP, LANES), F32),
         pltpu.VMEM((2, PAIRS, LANES), F32),
         pltpu.VMEM((ny, 2, PAIRS, LANES), F32),
-        pltpu.VMEM((2, PAIRS, LANES), F32),
-        pltpu.VMEM((nz, 2, PAIRS, LANES), F32),
+        pltpu.VMEM((2, 2, PAIRS, LANES), F32),
+        pltpu.VMEM((CHAIN, 2, PAIRS, LANES), F32),
         pltpu.VMEM((2, PAIRS, LANES), F32),
         pltpu.VMEM((PAIRS, ROWS, 2 * LANES), BF16),
         pltpu.VMEM((2, ROWS, LANES), F32),
@@ -498,39 +551,46 @@
         dma((12,)),
         dma((TP - 1,)),
         dma((TP - 1,)),
-        dma((ny - 1,)),
-        dma((ny - 1,)),
-        dma((nz - 1,)),
-        dma((nz - 1,)),
-        dma((14,)),
-        dma((14,)),
+        dma((max(ny - 1, 1),)),
+        dma((max(ny - 1, 1),)),
+        dma((CHAIN,)),
+        dma((CHAIN,)),
+        pltpu.SemaphoreType.REGULAR((CHAIN,)),
+        dma((16,)),
+        dma((16,)),
+        dma((5,)),
+        dma((5,)),
         dma((TP - 1,)),
         dma((TP - 1,)),
+    ]
+    operands = [
+        pltpu.with_memory_space_constraint(operand, pltpu.HBM)
+        for operand in (
+            tokens,
+            norm_in.reshape(1, D),
+            decay_log,
+            phase,
+            by_channel(b_real),
+            by_channel(b_imag),
+            c_real.reshape(WIDTH, STATE),
+            c_imag.reshape(WIDTH, STATE),
+            skip_gain.reshape(1, WIDTH),
+            w_value,
+            w_gate,
+            norm_out.reshape(1, WIDTH),
+        )
     ]
     return pl.pallas_call(
         functools.partial(kernel, nz, ny),
         out_shape=jax.ShapeDtypeStruct((ROWS, WIDTH), BF16),
-        in_specs=[pl.BlockSpec(memory_space=pl.ANY)] * 12,
+        in_specs=[pl.BlockSpec(memory_space=pltpu.HBM)] * 12,
         out_specs=pl.BlockSpec(memory_space=pltpu.VMEM),
         scratch_shapes=scratch,
         compiler_params=pltpu.CompilerParams(
             collective_id=0, has_side_effects=True, vmem_limit_bytes=48 * 1024 * 1024
         ),
         name="mixer",
-    )(
-        tokens,
-        norm_in.reshape(1, D),
-        decay_log,
-        phase,
-        by_channel(b_real),
-        by_channel(b_imag),
-        c_real.reshape(WIDTH, STATE),
-        c_imag.reshape(WIDTH, STATE),
-        skip_gain.reshape(1, WIDTH),
-        w_value,
-        w_gate,
-        norm_out.reshape(1, WIDTH),
-    )
+    )(*operands)
 
 
 def solution(mesh):

time: 58 us -> 38 us (0.66)
  the two profiles are of different devices: /device:TPU:65 before, /device:TPU:704 now
where the time goes in v2:
time: 38 us; the launch traced here: 37.8 us
  Pallas kernels  37.1 us (98%)
  local copies, waits for them, and re-layouts  0.64 us (2%)
    pallas_call x1, Pallas kernels, on_device(): pl.pallas_call(functools.partial(kernel, nz, ny), out_shape=jax.ShapeDtyp...  37.1 us

profile of v2, /device:TPU:704, one launch (start us, length us, event | category | flops | bytes accessed | tf_op | source)
XLA Modules:
  0.0 37.8 jit_solution(17693789577663832230)
XLA Ops:
  0.0 37.1 %mixer.1 = bf16[192,256]{1,0:T(8,128)(2,1)S(1)} custom-call(bf16[24,2048]{1,0:T(8,128)(2,1)} %tok.1, f32[1,2048]{1,0:T(1,128)} %bitcast.15, f32[16,64]{1,0:T(8,128)} %dl.1, f32[16,64]{1,0:T(8,128)} %ph.1, f32[256,64]{1,0:T(8,128)} %bitcast.11, f32[256,64]{1,0:T(8,128)} %bitcast.12, f32[256,64]{1,0:T(8,128)} %bitcast.13, f32[256,64]{1,0:T(8,128)} %bitcast.14, ...), custom_call_target="tpu_custom_call" | custom-call | tf_op jit(solution)/shard_map/mixer/pallas_call | solution.py:583
  37.2 0.6 %copy.14 = bf16[192,256]{1,0:T(8,128)(2,1)} copy(bf16[192,256]{1,0:T(8,128)(2,1)S(1)} %mixer.1) | data formatting | bytes 196608

commit v3 on v2

--- a/solution.py
+++ b/solution.py
@@ -26,6 +26,7 @@
 CHAIN = 4
 FAR_FIRST = (4, 3, 5, 2, 6, 1, 7)
 CHUNKS = 4
+ASKER, SCOUT = 1, 3
 MESH = pl.DeviceIdType.MESH
 
 
@@ -108,6 +109,8 @@
     zs_sem,
     zr_sem,
     here_sem,
+    go_sem,
+    asked_sem,
     gs_sem,
     gr_sem,
     ps_sem,
@@ -138,35 +141,42 @@
             )
         )
     ]
-    for load in loads[:4]:
+    for load in loads[:2]:
         load.start()
 
     barrier = pltpu.get_barrier_semaphore()
+    scout, asker = me == SCOUT, me == ASKER
+    knows_y = (me != 0) & (me != SCOUT)
+
+    def signal_tp(sem, peer):
+        pl.semaphore_signal(sem, inc=1, device_id={"tp": peer}, device_id_type=MESH)
+
+    def signal_y(sem, k):
+        pl.semaphore_signal(sem, inc=1, device_id={"sp_1": lax.rem(me_y + k, ny)}, device_id_type=MESH)
+
+    def signal_z(sem, k):
+        pl.semaphore_signal(sem, inc=1, device_id={"sp_0": me_z + k}, device_id_type=MESH)
+
     for k in FAR_FIRST:
-        pl.semaphore_signal(barrier, inc=1, device_id={"tp": lax.rem(me + k, TP)}, device_id_type=MESH)
-    for k in y_order:
-        pl.semaphore_signal(barrier, inc=1, device_id={"sp_1": lax.rem(me_y + k, ny)}, device_id_type=MESH)
-
-    @pl.when(me_z > 0)
+        signal_tp(barrier, lax.rem(me + k, TP))
+
+    @pl.when(knows_y)
     def _():
-        pl.semaphore_signal(barrier, inc=1, device_id={"sp_0": me_z - 1}, device_id_type=MESH)
-
-    @pl.when(me_z + 1 < nz)
-    def _():
-        pl.semaphore_signal(barrier, inc=1, device_id={"sp_0": me_z + 1}, device_id_type=MESH)
-
-    for load in loads[4:]:
+        for k in y_order:
+            signal_y(barrier, k)
+
+    pl.when(scout & (me_z > 0))(lambda: signal_z(barrier, -1))
+    pl.when(scout & (me_z + 1 < nz))(lambda: signal_z(barrier, 1))
+    for load in loads[2:]:
         load.start()
 
-    def tell(r):
-        @pl.when((me_z > 0) & (me_z + r < nz))
-        def _():
-            pl.semaphore_signal(here_sem.at[r - 1], inc=1, device_id={"sp_0": me_z - 1}, device_id_type=MESH)
-
-    def hear(r):
-        @pl.when(me_z + 1 + r < nz)
-        def _():
-            pl.semaphore_wait(here_sem.at[r - 1], 1)
+    def tell_z(r):
+        if r <= reach:
+            pl.when(scout & (me_z > 0) & (me_z + r - 1 < nz))(lambda: signal_z(here_sem.at[r - 1], -1))
+
+    def hear_z(r):
+        if r <= reach:
+            pl.when(scout & (me_z + r < nz))(lambda: pl.semaphore_wait(here_sem.at[r - 1], 1))
 
     loads[0].wait()
     loads[1].wait()
@@ -175,6 +185,25 @@
     normed = (x * lax.rsqrt(mean + NORM_EPS) * nin_v[...]).astype(BF16)
     for k in range(TP):
         xs[k] = normed[:, k * WIDTH : (k + 1) * WIDTH]
+
+    neighbours = jnp.minimum(me_z, 1) + jnp.minimum(nz - 1 - me_z, 1)
+    pl.semaphore_wait(barrier, TP - 1 + jnp.where(knows_y, ny - 1, 0) + jnp.where(scout, neighbours, 0))
+    tell_z(1)
+
+    @pl.when(asker)
+    def _():
+        for k in y_order:
+            signal_y(asked_sem.at[0], k)
+
+    xcopies = []
+    for k in FAR_FIRST:
+        peer = lax.rem(me + k, TP)
+        copy = pltpu.make_async_remote_copy(
+            xs.at[peer], xr.at[me], xs_sem.at[k - 1], xr_sem.at[k - 1], device_id={"tp": peer}, device_id_type=MESH
+        )
+        copy.start()
+        xcopies.append(copy)
+    xr[me] = xs[me]
 
     loads[2].wait()
     loads[3].wait()
@@ -212,28 +241,14 @@
     for g in range(GROUPS):
         split_store(wb, g, b_v[0, 16 * g : 16 * g + 16, :], b_v[1, 16 * g : 16 * g + 16, :])
 
-    neighbours = jnp.minimum(me_z, 1) + jnp.minimum(nz - 1 - me_z, 1)
-    pl.semaphore_wait(barrier, ny + TP - 2 + neighbours)
-    tell(1)
-
-    xcopies = []
-    for k in FAR_FIRST:
-        peer = lax.rem(me + k, TP)
-        copy = pltpu.make_async_remote_copy(
-            xs.at[peer], xr.at[me], xs_sem.at[k - 1], xr_sem.at[k - 1], device_id={"tp": peer}, device_id_type=MESH
-        )
-        copy.start()
-        xcopies.append(copy)
-    xr[me] = xs[me]
+    for r in range(1, 3):
+        hear_z(r)
+        tell_z(r + 1)
     for k in range(1, TP):
         source = lax.rem(me + TP - k, TP)
         pltpu.make_async_remote_copy(
             xs.at[source], xr.at[source], xs_sem.at[k - 1], xr_sem.at[k - 1], device_id={"tp": source}, device_id_type=MESH
         ).wait_recv()
-
-    if reach > 1:
-        hear(1)
-        tell(2)
 
     for j in range(TP):
         block = xr[j].astype(F32)
@@ -278,6 +293,7 @@
             es[k, pair : pair + 1, :] = total[k][TP - 1 : TP, :]
             fbuf[pair, k] = jnp.where(segment >= 1, pltpu.roll(total[k], 1, 0), 0.0)
 
+    pl.when(~knows_y)(lambda: pl.semaphore_wait(go_sem.at[0], 1))
     ycopies = []
     for k in y_order:
         peer = lax.rem(me_y + k, ny)
@@ -287,6 +303,22 @@
         copy.start()
         ycopies.append(copy)
     yr[me_y] = es[...]
+
+    @pl.when(asker)
+    def _():
+        if ny > 1:
+            pl.semaphore_wait(asked_sem.at[0], ny - 1)
+        signal_tp(go_sem.at[0], 0)
+        signal_tp(go_sem.at[0], SCOUT)
+
+    for r in range(3, reach + 1):
+        hear_z(r)
+        tell_z(r + 1)
+
+    @pl.when(scout)
+    def _():
+        for k in FAR_FIRST:
+            signal_tp(go_sem.at[1], (SCOUT + k) % TP)
 
     loads[6].wait()
     loads[7].wait()
@@ -322,11 +354,8 @@
         def _():
             zcopy(k, me_z + k).start()
 
-    zsend(1)
-    for k in range(2, min(reach, CHAIN - 1) + 1):
-        if k > 2:
-            hear(k - 1)
-            tell(k)
+    pl.when(me != SCOUT)(lambda: pl.semaphore_wait(go_sem.at[1], 1))
+    for k in range(min(reach, CHAIN - 1), 0, -1):
         zsend(k)
     held_v[...] = jnp.zeros_like(held_v)
     for k in range(reach, 0, -1):
@@ -339,7 +368,6 @@
 
     if reach == CHAIN:
         zs[1, 0], zs[1, 1] = cmuladd(line, (held_v[0], held_v[1]), total)
-        hear(CHAIN - 1)
         zsend(CHAIN)
     held = cmuladd((hop_v[me_y, 0], hop_v[me_y, 1]), (held_v[0], held_v[1]), inside)
     held_v[0], held_v[1] = held
@@ -556,6 +584,8 @@
         dma((CHAIN,)),
         dma((CHAIN,)),
         pltpu.SemaphoreType.REGULAR((CHAIN,)),
+        pltpu.SemaphoreType.REGULAR((2,)),
+        pltpu.SemaphoreType.REGULAR((1,)),
         dma((16,)),
         dma((16,)),
         dma((5,)),

time: 38 us -> 36 us (0.947)
  Pallas kernels: 37.1 us -> 35.2 us
    pallas_call x1, Pallas kernels: 37.1 us -> 35.2 us  [on_device(): pl.pallas_call(functools.partial(kernel, nz, ny), out_shape=jax.ShapeDtyp...]
where the time goes in v3:
time: 36 us; the launch traced here: 35.8 us
  Pallas kernels  35.2 us (98%)
  local copies, waits for them, and re-layouts  0.64 us (2%)
    pallas_call x1, Pallas kernels, on_device(): pl.pallas_call(functools.partial(kernel, nz, ny), out_shape=jax.ShapeDtyp...  35.2 us

profile of v3, /device:TPU:704, one launch (start us, length us, event | category | flops | bytes accessed | tf_op | source)
XLA Modules:
  0.0 35.8 jit_solution(4010577892774957085)
XLA Ops:
  0.0 35.2 %mixer.1 = bf16[192,256]{1,0:T(8,128)(2,1)S(1)} custom-call(bf16[24,2048]{1,0:T(8,128)(2,1)} %tok.1, f32[1,2048]{1,0:T(1,128)} %bitcast.15, f32[16,64]{1,0:T(8,128)} %dl.1, f32[16,64]{1,0:T(8,128)} %ph.1, f32[256,64]{1,0:T(8,128)} %bitcast.11, f32[256,64]{1,0:T(8,128)} %bitcast.12, f32[256,64]{1,0:T(8,128)} %bitcast.13, f32[256,64]{1,0:T(8,128)} %bitcast.14, ...), custom_call_target="tpu_custom_call" | custom-call | tf_op jit(solution)/shard_map/mixer/pallas_call | solution.py:613
  35.2 0.6 %copy.14 = bf16[192,256]{1,0:T(8,128)(2,1)} copy(bf16[192,256]{1,0:T(8,128)(2,1)S(1)} %mixer.1) | data formatting | bytes 196608
